TPU v7x, 32 devices: a whole 2x2x4 slice. The times are simulated.
32 devices in a mesh: grp: 2 (over y), kv: 4 (over z), tp: 4 (over x, core).
Axes of the slice: x: 2, y: 2, z: 4, core: 2. Of those that a mesh axis runs over, the one named last changes fastest.
Arguments:
- tokens: bfloat16 [176, 6, 4096], P(('grp', 'kv')), parts along dimension 0, may hold values from -6 to 6
- norm_gain: bfloat16 [4096], replicated, may hold values from 0.099609375 to 1.8984375
- w_query: bfloat16 [4096, 2048], P('kv', 'tp'), may hold values from -0.09375 to 0.09375
- w_key: bfloat16 [4096, 2048], P('kv', 'tp'), may hold values from -0.09375 to 0.09375
- w_value: bfloat16 [4096, 2048], P('kv', 'tp'), may hold values from -0.09375 to 0.09375
- w_igate: bfloat16 [4096, 16], P(None, 'tp'), may hold values from -0.09375 to 0.09375
- w_fgate: bfloat16 [4096, 16], P(None, 'tp'), may hold values from -0.09375 to 0.09375
- igate_bias: float32 [16], P('tp'), may hold values from -2 to 2
- fgate_bias: float32 [16], P('tp'), may hold values from 0.5 to 6
- head_gain: bfloat16 [2048], P('tp'), may hold values from 0.099609375 to 1.8984375
- w_out: bfloat16 [2048, 4096], P('tp', 'kv'), may hold values from -0.125 to 0.125
- state_matrix: float32 [176, 16, 128, 128], P(('grp', 'kv'), 'tp'), parts along dimension 0, may hold values from -1.5 to 1.5
- state_norm: float32 [176, 16, 128], P(('grp', 'kv'), 'tp'), parts along dimension 0, may hold values from -4 to 4
- state_max: float32 [176, 16], P(('grp', 'kv'), 'tp'), parts along dimension 0, may hold values from -4 to 4
- prior_keys: bfloat16 [176, 6, 2048], P(('grp', 'kv'), None, 'tp'), parts along dimension 0, may hold values from -6 to 6
- prior_values: bfloat16 [176, 6, 2048], P(('grp', 'kv'), None, 'tp'), parts along dimension 0, may hold values from -6 to 6
- prior_igate: float32 [176, 6, 16], P(('grp', 'kv'), None, 'tp'), parts along dimension 0, may hold values from -4 to 4
- prior_fgate: float32 [176, 6, 16], P(('grp', 'kv'), None, 'tp'), parts along dimension 0, may hold values from 0 to 5
- accepted: int32 [176], P(('grp', 'kv')), parts along dimension 0, may hold values from 0 to 6
Outputs:
- mixed: float32 [176, 6, 4096], P(('grp', 'kv'), None, 'tp'), parts along dimension 0
- new_matrix: float32 [176, 16, 128, 128], P(('grp', 'kv'), 'tp'), parts along dimension 0
- new_norm: float32 [176, 16, 128], P(('grp', 'kv'), 'tp'), parts along dimension 0
- new_max: float32 [176, 16], P(('grp', 'kv'), 'tp'), parts along dimension 0
There are 2 independent parts, one for each index of `grp`. A program takes and returns all parts, laid end to end along the dimension named above; an argument that names none is the same for every part. Nothing has to cross between parts.
Inputs may be any that keep to these rules, and one draw needn't show every extreme that they name: `accepted`: how many of the 6 proposals of the last step were kept, from the first on.
All inputs are finite; a program needn't handle non-finite values.
Results may differ from a plain program's by a relative error of at most 0.019.
Values may be sent and summed in bfloat16 or wider, within the bound.
A program may use at most 128 MiB of HBM per device.

v0:
```python
import jax
import jax.numpy as jnp
from jax import lax
from jax.sharding import PartitionSpec as P

EPS = 1e-06


def reduce_tiles(partial, axis_name, axis):
    size = lax.psum(1, axis_name)
    shape = partial.shape
    split = partial.astype(jnp.bfloat16).reshape(
        shape[:axis] + (size, shape[axis] // size) + shape[axis + 1 :]
    )
    split = jnp.moveaxis(split, axis, 0)
    got = lax.all_to_all(split, axis_name, split_axis=0, concat_axis=0, tiled=True)
    return jnp.sum(got.astype(jnp.float32), axis=0)


def bf_dot(spec, left, right):
    return jnp.einsum(
        spec,
        left.astype(jnp.bfloat16),
        right.astype(jnp.bfloat16),
        preferred_element_type=jnp.float32,
    )


def heads_first(array, heads):
    seqs_n, props, width = array.shape
    return (
        array.astype(jnp.float32)
        .reshape(seqs_n, props, heads, width // heads)
        .transpose(0, 2, 1, 3)
    )


def fold_prior(matrix, normer, stabil, keys, values, in_pre, forget_pre, accepted):
    positions = jnp.arange(keys.shape[2], dtype=jnp.int32)
    active_mask = positions[None, None, :] < accepted[:, None, None]
    log_forget = jnp.where(active_mask, jax.nn.log_sigmoid(forget_pre), 0.0)
    in_gate = jnp.where(active_mask, in_pre, -1e30)
    cum_forget = jnp.cumsum(log_forget, axis=-1)
    total_forget = cum_forget[..., -1]
    weight_log = total_forget[..., None] - cum_forget + in_gate
    new_stabil = jnp.maximum(total_forget + stabil, jnp.max(weight_log, axis=-1))
    carry_scale = jnp.exp(total_forget + stabil - new_stabil)
    weighted_keys = keys * jnp.exp(weight_log - new_stabil[..., None])[..., None]
    new_matrix = carry_scale[..., None, None] * matrix + bf_dot(
        "bhtd,bhte->bhde", weighted_keys, values
    )
    new_normer = carry_scale[..., None] * normer + jnp.sum(weighted_keys, axis=2)
    return (new_matrix, new_normer, new_stabil)


def read_block(matrix, normer, stabil, query, keys, values, in_pre, forget_pre):
    props = query.shape[2]
    cum_forget = jnp.cumsum(jax.nn.log_sigmoid(forget_pre), axis=-1)
    causal = jnp.tril(jnp.ones((props, props), jnp.bool_))
    log_decay = jnp.where(
        causal, cum_forget[..., :, None] - cum_forget[..., None, :] + in_pre[..., None, :], -1e30
    )
    inter = cum_forget + stabil[..., None]
    row_max = jnp.maximum(inter, jnp.max(log_decay, axis=-1))
    inter_scale = jnp.exp(inter - row_max)
    scores = bf_dot("bhtd,bhud->bhtu", query, keys)
    scores = scores * jnp.exp(log_decay - row_max[..., None])
    numerator = inter_scale[..., None] * bf_dot(
        "bhtd,bhde->bhte", query, matrix
    )
    numerator = numerator + bf_dot(
        "bhtu,bhue->bhte", scores, values
    )
    denominator = inter_scale * jnp.sum(query * normer[:, :, None, :], axis=-1)
    denominator = denominator + jnp.sum(scores, axis=-1)
    return numerator / jnp.maximum(jnp.abs(denominator), jnp.exp(-row_max))[..., None]


def head_norm(cell, head_gain):
    seqs_n, heads, props, width = cell.shape
    scaled = cell * lax.rsqrt(jnp.mean(cell * cell, axis=-1, keepdims=True) + EPS)
    scaled = scaled.transpose(0, 2, 1, 3).reshape(seqs_n * props, heads * width)
    return (scaled * head_gain.astype(jnp.float32)).astype(jnp.bfloat16)


def body(
    tokens,
    norm_gain,
    w_query,
    w_key,
    w_value,
    w_igate,
    w_fgate,
    igate_bias,
    fgate_bias,
    head_gain,
    w_out,
    state_matrix,
    state_norm,
    state_max,
    prior_keys,
    prior_values,
    prior_igate,
    prior_fgate,
    accepted,
):
    seq_count, props, width = tokens.shape
    local_heads = state_matrix.shape[1]
    key_size = state_matrix.shape[2]
    row_count = seq_count * props
    inputs = tokens.astype(jnp.float32)
    normed = inputs * lax.rsqrt(jnp.mean(inputs * inputs, axis=-1, keepdims=True) + EPS)
    normed_rows = (
        (normed * norm_gain.astype(jnp.float32)).astype(jnp.bfloat16).reshape(row_count, width)
    )
    query_width = w_query.shape[1]
    combined = jnp.concatenate([w_query, w_key, w_value], axis=1)
    received = lax.all_to_all(normed_rows, "kv", split_axis=1, concat_axis=0, tiled=True)
    summed = reduce_tiles(
        jnp.dot(received, combined, preferred_element_type=jnp.float32), "kv", 0
    )
    query_sum = summed[:, :query_width]
    key_sum = summed[:, query_width : 2 * query_width]
    value_sum = summed[:, 2 * query_width :]
    query = query_sum.astype(jnp.bfloat16).reshape(seq_count, props, -1)
    keys = key_sum.astype(jnp.bfloat16).reshape(seq_count, props, -1)
    values = value_sum.astype(jnp.bfloat16).reshape(seq_count, props, -1)
    in_pre = jnp.dot(normed_rows, w_igate, preferred_element_type=jnp.float32) + igate_bias
    forget_pre = jnp.dot(normed_rows, w_fgate, preferred_element_type=jnp.float32) + fgate_bias
    in_pre = in_pre.reshape(seq_count, props, local_heads).transpose(0, 2, 1)
    forget_pre = forget_pre.reshape(seq_count, props, local_heads).transpose(0, 2, 1)
    new_matrix, new_normer, new_stabil = fold_prior(
        state_matrix,
        state_norm,
        state_max,
        heads_first(prior_keys, local_heads) * key_size ** (-0.5),
        heads_first(prior_values, local_heads),
        prior_igate.transpose(0, 2, 1),
        prior_fgate.transpose(0, 2, 1),
        accepted,
    )
    cell = read_block(
        new_matrix,
        new_normer,
        new_stabil,
        heads_first(query, local_heads),
        heads_first(keys, local_heads) * key_size ** (-0.5),
        heads_first(values, local_heads),
        in_pre,
        forget_pre,
    )
    hidden = head_norm(cell, head_gain)
    partial_out = jnp.dot(
        hidden, lax.all_gather(w_out, "kv", axis=1, tiled=True), preferred_element_type=jnp.float32
    )
    mixed = reduce_tiles(partial_out, "tp", 1)
    return (mixed.reshape(seq_count, props, -1), new_matrix, new_normer, new_stabil)


def solution(mesh):
    return jax.shard_map(
        body,
        mesh=mesh,
        in_specs=(
            P(("grp", "kv"), None, None),
            P(),
            P("kv", "tp"),
            P("kv", "tp"),
            P("kv", "tp"),
            P(None, "tp"),
            P(None, "tp"),
            P("tp"),
            P("tp"),
            P("tp"),
            P("tp", "kv"),
            P(("grp", "kv"), "tp", None, None),
            P(("grp", "kv"), "tp", None),
            P(("grp", "kv"), "tp"),
            P(("grp", "kv"), None, "tp"),
            P(("grp", "kv"), None, "tp"),
            P(("grp", "kv"), None, "tp"),
            P(("grp", "kv"), None, "tp"),
            P(("grp", "kv")),
        ),
        out_specs=(
            P(("grp", "kv"), None, "tp"),
            P(("grp", "kv"), "tp", None, None),
            P(("grp", "kv"), "tp", None),
            P(("grp", "kv"), "tp"),
        ),
        check_vma=False,
    )
```

profile of v0, /device:TPU:1, one launch (start us, length us, event | category | flops | bytes accessed | tf_op | source)
XLA Modules:
  0.0 186.7 jit_solution(5090905955651514263)
XLA Ops:
  7.2 1.6 fusion.11
  8.8 0.7 convert_element_type.85
  9.5 1.6 fusion.13
  11.1 0.6 copy.136
  11.8 1.5 all_to_all.20
  13.3 1.3 copy.148
  14.6 5.4 %all-to-all-start = ((bf16[132,4,1024]{2,0,1:T(8,128)(2,1)}), bf16[132,4,1024]{2,0,1:T(8,128)(2,1)S(1)}, u32[]{:S(2)}, u32[]{:S(2)}) async-start(bf16[132,4,1024]{2,0,1:T(8,128)(2,1)} %copy.148), calls=%async_computation | async-start | bytes 2228224 | tf_op jit(solution)/shard_map/all_to_all | solution.py:118
  20.1 0.7 all-gather.2.cloned.1.call-update
  20.9 41.9 %all-to-all-done = bf16[132,4,1024]{2,0,1:T(8,128)(2,1)S(1)} async-done(((bf16[132,4,1024]{2,0,1:T(8,128)(2,1)}), bf16[132,4,1024]{2,0,1:T(8,128)(2,1)S(1)}, u32[]{:S(2)}, u32[]{:S(2)}) %all-to-all-start) | async-done | bytes 1081376 | tf_op jit(solution)/shard_map/all_to_all | solution.py:118
  62.8 1.1 all_to_all.23
  63.9 4.1 %fusion.6 = bf16[528,1536]{1,0:T(8,128)(2,1)S(1)} fusion(bf16[528,1024]{1,0:T(8,128)(2,1)} %all_to_all.23, bf16[1024,512]{1,0:T(8,128)(2,1)} %param.23, bf16[1024,512]{1,0:T(8,128)(2,1)} %param.22, bf16[1024,512]{1,0:T(8,128)(2,1)} %param.21), kind=kOutput, calls=%fused_computation.8 | convolution fusion | flops 1671192576 | bytes 5849088 | tf_op jit(solution)/shard_map/dot_general | solution.py:120
  67.9 1.4 reshape.132
  69.3 4.7 %all-to-all-start.1 = ((bf16[4,132,1536]{2,1,0:T(8,128)(2,1)}), bf16[4,132,1536]{2,1,0:T(8,128)(2,1)}, u32[]{:S(2)}, u32[]{:S(2)}) async-start(bf16[4,132,1536]{2,1,0:T(8,128)(2,1)} %reshape.132), calls=%async_computation.1 | async-start | bytes 3342336 | tf_op jit(solution)/shard_map/all_to_all | solution.py:16
  74.1 0.1 copy.138
  74.2 0.4 reshape.130
  74.6 0.1 copy.170
  74.9 0.1 reshape.137
  75.1 0.4 fusion.14
  75.4 0.1 neg.42
  75.6 0.1 copy.137
  75.7 0.1 copy.142
  75.8 0.4 convolution_add_fusion
  76.2 0.1 reshape.131
  76.4 0.3 fusion.19
  76.7 0.1 copy.145
  76.8 0.1 copy.151
  76.9 0.1 copy.155
  77.0 0.2 fusion.17
  77.4 7.5 %multiply_add_fusion = f32[22,4,128,128]{3,2,1,0:T(8,128)} fusion(f32[22,4,128,128]{3,2,1,0:T(8,128)} %param.30, f32[22,4]{1,0:T(8,128)S(1)} %get-tuple-element.26, f32[22,6,4,128]{3,2,0,1:T(4,128)S(1)} %reshape.137, bf16[22,6,4,128]{3,2,0,1:T(4,128)(2,1)S(1)} %convert_element_type.92, f32[22,4,6]{2,1,0:T(4,128)S(1)} %copy.151), kind=kOutput, calls=%fused_computation | convolution fusion | flops 20320256 | bytes 11942304 | tf_op jit(solution)/shard_map/bhtd,bhte->bhde/dot_general | solution.py:21
  84.9 61.7 %all-to-all-done.1 = bf16[4,132,1536]{2,1,0:T(8,128)(2,1)} async-done(((bf16[4,132,1536]{2,1,0:T(8,128)(2,1)}), bf16[4,132,1536]{2,1,0:T(8,128)(2,1)}, u32[]{:S(2)}, u32[]{:S(2)}) %all-to-all-start.1) | async-done | bytes 1622048 | tf_op jit(solution)/shard_map/all_to_all | solution.py:16
  146.6 1.7 reduce.1
  148.5 0.4 fusion.71
  148.9 0.1 copy.159
  149.0 0.2 multiply_reduce_fusion.1
  149.2 0.1 copy.158
  149.4 0.1 copy.164
  149.5 0.1 copy.146
  149.6 0.1 copy.161
  149.7 0.1 copy.160
  149.9 3.5 %fusion.9 = f32[22,4,6,128]{3,2,1,0:T(8,128)S(1)} fusion(f32[22,4,128,128]{3,2,1,0:T(8,128)} %multiply_add_fusion, bf16[22,6,4,128]{3,2,1,0:T(4,128)(2,1)S(1)} %convert_element_type.89), kind=kOutput, calls=%fused_computation.11 | convolution fusion | flops 18743296 | bytes 6172672 | tf_op jit(solution)/shard_map/bhtd,bhde->bhte/dot_general | solution.py:21
  153.4 0.5 multiply_reduce_fusion
  154.0 0.3 fusion.16
  154.5 2.9 %convolution_convert_fusion = bf16[132,4096]{1,0:T(8,128)(2,1)S(1)} fusion(bf16[512,4096]{1,0:T(8,128)(2,1)} %all-gather.2.cloned.1.call-done, f32[132,512]{1,0:T(8,128)S(1)} %bitcast.148, f32[512]{0:T(512)S(1)} %convert_element_type.103), kind=kOutput, calls=%fused_computation.1 | convolution fusion | flops 554323968 | bytes 5548032 | tf_op jit(solution)/shard_map/dot_general | solution.py:153
  157.5 0.6 reshape.135
  158.1 0.3 copy.205
  158.4 20.0 %all_to_all.29 = bf16[4,132,1024]{2,1,0:T(8,128)(2,1)S(1)} all-to-all(bf16[4,132,1024]{2,1,0:T(8,128)(2,1)S(1)} %bitcast.147), channel_id=1, replica_groups=mesh['grp'=2,'kv'=4,'tp'=4] {'tp'}, dimensions={0} | all-to-all | bytes 2162688 | tf_op jit(solution)/shard_map/all_to_all | solution.py:16
  178.4 0.2 convert_reduce_fusion
  178.7 1.1 copy.167
  (57 shorter events, 1.0 us)
Async XLA Ops:
  7.2 67.9 %copy-start = (bf16[4096,4]{0,1:T(4,128)(2,1)S(1)}, bf16[4096,4]{0,1:T(4,128)(2,1)}, u32[]{:S(2)}) copy-start(bf16[4096,4]{0,1:T(4,128)(2,1)} %param.25) | copy-start | bytes 98308
  13.3 7.5 %copy-start.13 = (s32[22]{0:T(128)S(1)}, s32[22]{0:T(128)}, u32[]{:S(2)}) copy-start(s32[22]{0:T(128)} %param.37) | copy-start | bytes 268
  13.3 7.5 %copy-start.8 = (f32[22,6,4]{0,2,1:T(4,128)S(1)}, f32[22,6,4]{0,2,1:T(4,128)}, u32[]{:S(2)}) copy-start(f32[22,6,4]{0,2,1:T(4,128)} %param.36) | copy-start | bytes 6340
  14.6 48.1 %all-to-all-start = ((bf16[132,4,1024]{2,0,1:T(8,128)(2,1)}), bf16[132,4,1024]{2,0,1:T(8,128)(2,1)S(1)}, u32[]{:S(2)}, u32[]{:S(2)}) async-start(bf16[132,4,1024]{2,0,1:T(8,128)(2,1)} %copy.148), calls=%async_computation | async-start | bytes 2228224 | tf_op jit(solution)/shard_map/all_to_all | solution.py:118
  20.1 134.5 %all-gather.2.cloned.1.call-start = ((), (), s32[]{:S(2)}) async-start(), calls=%async_computation.3 | async-start | bytes 5242880 | tf_op jit(solution)/shard_map/all_gather | solution.py:154
  69.3 4.7 %copy-start.4 = (f32[22,6,4]{0,2,1:T(4,128)S(1)}, f32[22,6,4]{0,2,1:T(4,128)}, u32[]{:S(2)}) copy-start(f32[22,6,4]{0,2,1:T(4,128)} %param.35) | copy-start | bytes 6340
  69.3 5.2 %copy-start.10 = (bf16[512]{0:T(512)(128)(2,1)S(1)}, bf16[512]{0:T(512)(128)(2,1)}, u32[]{:S(2)}) copy-start(bf16[512]{0:T(512)(128)(2,1)} %param.28) | copy-start | bytes 3076
  69.3 5.4 %copy-start.9 = (f32[22,4]{0,1:T(4,128)S(1)}, f32[22,4]{0,1:T(4,128)}, u32[]{:S(2)}) copy-start(f32[22,4]{0,1:T(4,128)} %param.32) | copy-start | bytes 1060
  69.3 5.6 %copy-start.3 = (bf16[22,6,512]{2,0,1:T(8,128)(2,1)S(1)}, bf16[22,6,512]{2,0,1:T(8,128)(2,1)}, u32[]{:S(2)}) copy-start(bf16[22,6,512]{2,0,1:T(8,128)(2,1)} %param.34) | copy-start | bytes 405508
  69.3 5.6 %copy-start.2 = (bf16[22,6,512]{2,0,1:T(8,128)(2,1)S(1)}, bf16[22,6,512]{2,0,1:T(8,128)(2,1)}, u32[]{:S(2)}) copy-start(bf16[22,6,512]{2,0,1:T(8,128)(2,1)} %param.33) | copy-start | bytes 405508
  69.3 77.3 %all-to-all-start.1 = ((bf16[4,132,1536]{2,1,0:T(8,128)(2,1)}), bf16[4,132,1536]{2,1,0:T(8,128)(2,1)}, u32[]{:S(2)}, u32[]{:S(2)}) async-start(bf16[4,132,1536]{2,1,0:T(8,128)(2,1)} %reshape.132), calls=%async_computation.1 | async-start | bytes 3342336 | tf_op jit(solution)/shard_map/all_to_all | solution.py:16
  74.0 1.0 copy-start.11
  74.2 1.7 copy-start.6
  74.2 1.7 copy-start.12
  74.5 2.7 %copy-start.5 = (f32[22,4,128]{2,1,0:T(4,128)S(1)}, f32[22,4,128]{2,1,0:T(4,128)}, u32[]{:S(2)}) copy-start(f32[22,4,128]{2,1,0:T(4,128)} %param.31) | copy-start | bytes 135172
  74.9 74.6 %copy-start.7 = (f32[22,4]{0,1:T(4,128)}, f32[22,4]{0,1:T(4,128)S(1)}, u32[]{:S(2)}) copy-start(f32[22,4]{0,1:T(4,128)S(1)} %copy.141) | copy-start | bytes 1060
  77.4 71.6 %copy-start.1 = (f32[22,4,128]{2,1,0:T(4,128)}, f32[22,4,128]{2,1,0:T(4,128)S(1)}, u32[]{:S(2)}) copy-start(f32[22,4,128]{2,1,0:T(4,128)S(1)} %multiply_add_fusion.1) | copy-start | bytes 135172
Sparse Core Ops, SparseCore 0:
  22.4 128.9 all-gather.1
where the time goes:
time: 188 us; the launch traced here: 187 us
  waiting for transfers between devices  104 us (55%)
  blocking collectives  20 us (11%)
  matrix products  19.7 us (10%)
  between operations  14.4 us (8%)
  local copies, waits for them, and re-layouts  10.9 us (6%)
  starting transfers between devices  10.1 us (5%)
  other arithmetic  7.25 us (4%)
    all_to_all x1, waiting for transfers between devices, reduce_tiles(): lax.all_to_all(split, axis_name, split_axis=0, concat_axis=0, tiled=True)  61.7 us
    all_to_all x1, waiting for transfers between devices, body(): lax.all_to_all(normed_rows, 'kv', split_axis=1, concat_axis=0, tiled=True)  41.9 us
    all_to_all x1, blocking collectives, reduce_tiles(): lax.all_to_all(split, axis_name, split_axis=0, concat_axis=0, tiled=True)  20 us
    dot_general x4, matrix products, bf_dot(): jnp.einsum(spec, left.astype(jnp.bfloat16), right.astype(jnp.bfloat16), p...  11.9 us
    all_to_all x1, starting transfers between devices, body(): lax.all_to_all(normed_rows, 'kv', split_axis=1, concat_axis=0, tiled=True)  5.41 us
    all_to_all x1, starting transfers between devices, reduce_tiles(): lax.all_to_all(split, axis_name, split_axis=0, concat_axis=0, tiled=True)  4.69 us
    dot_general x1, matrix products, body(): jnp.dot(received, combined, preferred_element_type=jnp.float32)  4.06 us
    all_to_all x3, local copies, waits for them, and re-layouts, body(): lax.all_to_all(normed_rows, 'kv', split_axis=1, concat_axis=0, tiled=True)  3.94 us
  transfers between devices with their start and end apart: 3, of which 2 were waited for; matrix products, arithmetic and copies ran while one was open for 13% of the time, Pallas kernels for 0%

commit v1 on v0

--- a/solution.py
+++ b/solution.py
@@ -1,9 +1,450 @@
+import functools
+
 import jax
 import jax.numpy as jnp
 from jax import lax
+from jax.experimental import pallas as pl
+from jax.experimental.pallas import tpu as pltpu
 from jax.sharding import PartitionSpec as P
 
 EPS = 1e-06
+MESH = pl.DeviceIdType.MESH
+
+
+def greet_all(kv_size, tp_size):
+    z, t = lax.axis_index("kv"), lax.axis_index("tp")
+    barrier = pltpu.get_barrier_semaphore()
+    for dz in range(kv_size):
+        for dt in range(tp_size):
+            if dz or dt:
+                pl.semaphore_signal(
+                    barrier,
+                    1,
+                    device_id={"kv": lax.rem(z + dz, kv_size), "tp": lax.rem(t + dt, tp_size)},
+                    device_id_type=MESH,
+                )
+    pl.semaphore_wait(barrier, kv_size * tp_size - 1)
+
+
+def other_at(index, z, kv_size):
+    right = kv_size - 1 - z
+    near, far = jnp.minimum(z, right), jnp.maximum(z, right)
+    single = far - near
+    later = index - single
+    both = jnp.where(later % 2 == 0, z + near - later // 2, z - near + later // 2)
+    lone = jnp.where(right > z, z + far - index, z - far + index)
+    return jnp.where(index < single, lone, both)
+
+
+def merged_away(source, j, kv_size):
+    inner = jnp.logical_and(j > 0, j < kv_size - 1)
+    return jnp.logical_and(inner, jnp.abs(source - j) == 2)
+
+
+def row_chunks(rows, count):
+    step = -(-(-(-rows // count)) // 8) * 8
+    return [(at, min(step, rows - at)) for at in range(0, rows, step)]
+
+
+def remote(src, dst, send, recv, kv, tp):
+    return pltpu.make_async_remote_copy(
+        src_ref=src,
+        dst_ref=dst,
+        send_sem=send,
+        recv_sem=recv,
+        device_id={"kv": kv, "tp": tp},
+        device_id_type=MESH,
+    )
+
+
+def project_kernel(
+    kv_size,
+    tp_size,
+    chunks,
+    normed_ref,
+    wq_ref,
+    wk_ref,
+    wv_ref,
+    out_ref,
+    rows_in,
+    weights,
+    own_sum,
+    partial,
+    outgoing,
+    incoming,
+    merging,
+    weight_sem,
+    a_send,
+    a_recv,
+    f_send,
+    f_recv,
+    b_send,
+    b_recv,
+    m_recv,
+):
+    z, t = lax.axis_index("kv"), lax.axis_index("tp")
+    depth = weights.shape[0]
+    part = depth // tp_size
+    width = wq_ref.shape[1]
+    others = kv_size - 1
+    loads = [
+        pltpu.make_async_copy(ref, weights.at[:, pl.ds(at * width, width)], weight_sem.at[at])
+        for at, ref in enumerate((wq_ref, wk_ref, wv_ref))
+    ]
+    for load in loads:
+        load.start()
+    greet_all(kv_size, tp_size)
+
+    def mine(at):
+        return pl.ds(pl.multiple_of(at * part, part), part)
+
+    def first_copy(j, source):
+        columns = pl.ds(pl.multiple_of(j * depth + t * part, part), part)
+        return remote(
+            normed_ref.at[:, columns], rows_in.at[source, :, mine(t)], a_send.at[j], a_recv.at[source], j, t
+        )
+
+    def forward_copy(j, source, dt):
+        peer = lax.rem(t + dt, tp_size)
+        return remote(
+            rows_in.at[j, :, mine(source)],
+            rows_in.at[j, :, mine(source)],
+            f_send.at[j, dt],
+            f_recv.at[j, source],
+            z,
+            peer,
+        )
+
+    def start_first(index, carry):
+        first_copy(other_at(index, z, kv_size), z).start()
+        return carry
+
+    lax.fori_loop(0, others, start_first, 0)
+    for load in loads:
+        load.wait()
+    own_columns = pl.ds(pl.multiple_of(z * depth, depth), depth)
+    for at, count in chunks:
+        own_sum[pl.ds(at, count), :] = jnp.dot(
+            normed_ref[pl.ds(at, count), own_columns], weights[...], preferred_element_type=jnp.float32
+        )
+
+    def forward(index, carry):
+        j = other_at(index, z, kv_size)
+        first_copy(z, j).wait_recv()
+        for dt in range(1, tp_size):
+            forward_copy(j, t, dt).start()
+        return carry
+
+    lax.fori_loop(0, others, forward, 0)
+
+    def merge_copy(j, number, rows):
+        way = jnp.where(j > z, 1, 0)
+        middle = jnp.where(j > z, z + 1, z - 1)
+        return remote(
+            outgoing.at[j, rows, :],
+            merging.at[way, rows, :],
+            b_send.at[j, number],
+            m_recv.at[way, number],
+            middle,
+            t,
+        )
+
+    def sum_copy(j, source, number, rows):
+        return remote(
+            outgoing.at[j, rows, :],
+            incoming.at[source, rows, :],
+            b_send.at[j, number],
+            b_recv.at[source, number],
+            j,
+            t,
+        )
+
+    def unit(number, at, count, index):
+        j = other_at(index, z, kv_size)
+        way = jnp.where(j > z, 1, 0)
+        behind = 2 * z - j
+        merges = jnp.logical_and(behind >= 0, behind < kv_size)
+        merges = jnp.logical_and(merges, merged_away(behind, j, kv_size))
+        if number == 0:
+            for dt in range(1, tp_size):
+                forward_copy(j, lax.rem(t + dt, tp_size), dt).wait_recv()
+        rows = pl.ds(at, count)
+        partial[pl.ds(0, count), :] = jnp.dot(
+            rows_in[j, rows, :], weights[...], preferred_element_type=jnp.float32
+        )
+
+        @pl.when(merges)
+        def _():
+            merge_copy(j, number, rows).wait_recv()
+            partial[pl.ds(0, count), :] += merging[way, rows, :].astype(jnp.float32)
+
+        outgoing[j, rows, :] = partial[pl.ds(0, count), :].astype(jnp.bfloat16)
+        away = merged_away(z, j, kv_size)
+
+        @pl.when(away)
+        def _():
+            merge_copy(j, number, rows).start()
+
+        @pl.when(jnp.logical_not(away))
+        def _():
+            sum_copy(j, z, number, rows).start()
+
+    for number, (at, count) in enumerate(chunks):
+
+        def run(index, carry, number=number, at=at, count=count):
+            unit(number, at, count, index)
+            return carry
+
+        lax.fori_loop(0, others, run, 0)
+
+    for number, (at, count) in enumerate(chunks):
+        rows = pl.ds(at, count)
+
+        def add(index, carry, rows=rows, number=number):
+            j = other_at(index, z, kv_size)
+
+            @pl.when(jnp.logical_not(merged_away(j, z, kv_size)))
+            def _():
+                sum_copy(z, j, number, rows).wait_recv()
+                own_sum[rows, :] += incoming[j, rows, :].astype(jnp.float32)
+
+            return carry
+
+        lax.fori_loop(0, others, add, 0)
+        out_ref[rows, :] = own_sum[rows, :].astype(jnp.bfloat16)
+
+    def drain(index, carry):
+        j = other_at(index, z, kv_size)
+        first_copy(j, z).wait_send()
+        for dt in range(1, tp_size):
+            forward_copy(j, t, dt).wait_send()
+        for number, (at, count) in enumerate(chunks):
+            sum_copy(j, z, number, pl.ds(at, count)).wait_send()
+        return carry
+
+    lax.fori_loop(0, others, drain, 0)
+
+
+def project(normed_rows, w_query, w_key, w_value, kv_size, tp_size):
+    rows, width = normed_rows.shape
+    depth = width // kv_size
+    columns = 3 * w_query.shape[1]
+    chunks = row_chunks(rows, 3)
+    sem = pltpu.SemaphoreType.DMA
+    hbm = pl.BlockSpec(memory_space=pl.ANY)
+    return pl.pallas_call(
+        functools.partial(project_kernel, kv_size, tp_size, chunks),
+        out_shape=jax.ShapeDtypeStruct((rows, columns), jnp.bfloat16),
+        in_specs=[pl.BlockSpec(memory_space=pltpu.VMEM), hbm, hbm, hbm],
+        out_specs=pl.BlockSpec(memory_space=pltpu.VMEM),
+        scratch_shapes=[
+            pltpu.VMEM((kv_size, rows, depth), jnp.bfloat16),
+            pltpu.VMEM((depth, columns), jnp.bfloat16),
+            pltpu.VMEM((rows, columns), jnp.float32),
+            pltpu.VMEM((chunks[0][1], columns), jnp.float32),
+            pltpu.VMEM((kv_size, rows, columns), jnp.bfloat16),
+            pltpu.VMEM((kv_size, rows, columns), jnp.bfloat16),
+            pltpu.VMEM((2, rows, columns), jnp.bfloat16),
+            sem((3,)),
+            sem((kv_size,)),
+            sem((kv_size,)),
+            sem((kv_size, tp_size)),
+            sem((kv_size, tp_size)),
+            sem((kv_size, len(chunks))),
+            sem((kv_size, len(chunks))),
+            sem((2, len(chunks))),
+        ],
+        compiler_params=pltpu.CompilerParams(
+            collective_id=0, has_side_effects=True, vmem_limit_bytes=60 * 1024 * 1024
+        ),
+    )(normed_rows, w_query, w_key, w_value)
+
+
+def output_kernel(
+    kv_size,
+    tp_size,
+    stages,
+    hidden_ref,
+    w_ref,
+    out_ref,
+    hidden_in,
+    weights,
+    sums,
+    landed,
+    *rest,
+):
+    halves = rest[: 2 * stages]
+    weight_sem, h_send, h_recv, r_send, r_recv, o_send, o_recv, outgoing = rest[2 * stages :]
+    z, t = lax.axis_index("kv"), lax.axis_index("tp")
+    others = kv_size - 1
+    width = weights.shape[1]
+    piece = width // tp_size
+    load = pltpu.make_async_copy(w_ref, weights, weight_sem.at[0])
+    load.start()
+    greet_all(kv_size, tp_size)
+
+    def hidden_copy(j, source):
+        return remote(hidden_ref, hidden_in.at[source], h_send.at[j], h_recv.at[source], j, t)
+
+    def start_hidden(index, carry):
+        hidden_copy(other_at(index, z, kv_size), z).start()
+        return carry
+
+    lax.fori_loop(0, others, start_hidden, 0)
+    load.wait()
+
+    def half_copy(j, stage):
+        peer = jnp.bitwise_xor(t, 1 << stage)
+        return remote(
+            halves[2 * stage].at[j],
+            halves[2 * stage + 1].at[j],
+            r_send.at[j, stage],
+            r_recv.at[j, stage],
+            z,
+            peer,
+        )
+
+    def split(j, stage, low, high):
+        bit = jnp.bitwise_and(lax.shift_right_logical(t, stage), 1)
+
+        @pl.when(bit == 0)
+        def _():
+            halves[2 * stage][j] = high().astype(jnp.bfloat16)
+
+        @pl.when(bit == 1)
+        def _():
+            halves[2 * stage][j] = low().astype(jnp.bfloat16)
+
+        half_copy(j, stage).start()
+
+    def bit_of(stage):
+        return jnp.bitwise_and(lax.shift_right_logical(t, stage), 1)
+
+    def first_stage(j, block):
+        sums[j] = jnp.dot(block, weights[...], preferred_element_type=jnp.float32)
+        split(
+            j,
+            0,
+            lambda: sums[j, :, pl.ds(0, width // 2)],
+            lambda: sums[j, :, pl.ds(width // 2, width // 2)],
+        )
+
+    def each(function):
+        def run(index, carry):
+            function(jnp.where(index == others, z, other_at(jnp.minimum(index, others - 1), z, kv_size)))
+            return carry
+
+        lax.fori_loop(0, kv_size, run, 0)
+
+    first_stage(z, hidden_ref[...])
+
+    def near_first(index, carry):
+        j = other_at(others - 1 - index, z, kv_size)
+        hidden_copy(z, j).wait_recv()
+        first_stage(j, hidden_in[j])
+        return carry
+
+    lax.fori_loop(0, others, near_first, 0)
+
+    offset = 0
+    for stage in range(stages):
+        size = width >> (stage + 1)
+        offset = offset + bit_of(stage) * size
+
+        def gather(j, stage=stage, size=size, offset=offset):
+            half_copy(j, stage).wait_recv()
+            kept = pl.ds(pl.multiple_of(offset, size), size)
+            sums[j, :, kept] += halves[2 * stage + 1][j].astype(jnp.float32)
+            if stage + 1 < stages:
+                small = size // 2
+                split(
+                    j,
+                    stage + 1,
+                    lambda: sums[j, :, pl.ds(pl.multiple_of(offset, small), small)],
+                    lambda: sums[j, :, pl.ds(pl.multiple_of(offset + small, small), small)],
+                )
+            else:
+                outgoing[j] = sums[j, :, kept].astype(jnp.bfloat16)
+
+                @pl.when(jnp.logical_or(j != z, t != z))
+                def _():
+                    final_copy(j).start()
+
+        def final_copy(j):
+            return remote(outgoing.at[j], landed.at[t], o_send.at[j], o_recv.at[t], j, z)
+
+        each(gather)
+
+    for sender in range(tp_size):
+        at = sum(((sender >> stage) & 1) * (width >> (stage + 1)) for stage in range(stages))
+        columns = pl.ds(at, piece)
+        local = jnp.logical_and(z == t, t == sender)
+
+        @pl.when(local)
+        def _(columns=columns):
+            out_ref[:, columns] = outgoing[z].astype(jnp.float32)
+
+        @pl.when(jnp.logical_not(local))
+        def _(columns=columns, sender=sender):
+            remote(landed.at[sender], landed.at[sender], o_send.at[0], o_recv.at[sender], z, t).wait_recv()
+            out_ref[:, columns] = landed[sender].astype(jnp.float32)
+
+    def drain(index, carry):
+        hidden_copy(other_at(index, z, kv_size), z).wait_send()
+        return carry
+
+    lax.fori_loop(0, others, drain, 0)
+
+    def drain_each(j):
+        for stage in range(stages):
+            half_copy(j, stage).wait_send()
+
+        @pl.when(jnp.logical_or(j != z, t != z))
+        def _():
+            remote(outgoing.at[j], landed.at[t], o_send.at[j], o_recv.at[t], j, z).wait_send()
+
+    each(drain_each)
+
+
+def output(hidden, w_out, kv_size, tp_size):
+    rows, heads_width = hidden.shape
+    width = w_out.shape[1]
+    stages = tp_size.bit_length() - 1
+    sem = pltpu.SemaphoreType.DMA
+    halves = []
+    for stage in range(stages):
+        halves += [pltpu.VMEM((kv_size, rows, width >> (stage + 1)), jnp.bfloat16)] * 2
+    piece = width // tp_size
+    return pl.pallas_call(
+        functools.partial(output_kernel, kv_size, tp_size, stages),
+        out_shape=jax.ShapeDtypeStruct((rows, width), jnp.float32),
+        in_specs=[pl.BlockSpec(memory_space=pltpu.VMEM), pl.BlockSpec(memory_space=pl.ANY)],
+        out_specs=pl.BlockSpec(memory_space=pltpu.VMEM),
+        scratch_shapes=[
+            pltpu.VMEM((kv_size, rows, heads_width), jnp.bfloat16),
+            pltpu.VMEM((heads_width, width), jnp.bfloat16),
+            pltpu.VMEM((kv_size, rows, width), jnp.float32),
+            pltpu.VMEM((tp_size, rows, piece), jnp.bfloat16),
+            *halves,
+            sem((1,)),
+            sem((kv_size,)),
+            sem((kv_size,)),
+            sem((kv_size, stages)),
+            sem((kv_size, stages)),
+            sem((kv_size,)),
+            sem((tp_size,)),
+            pltpu.VMEM((kv_size, rows, piece), jnp.bfloat16),
+        ],
+        compiler_params=pltpu.CompilerParams(
+            collective_id=1, has_side_effects=True, vmem_limit_bytes=60 * 1024 * 1024
+        ),
+    )(hidden, w_out)
+
+
+def kernels_fit(kv_size, tp_size, width, out_width):
+    powers = kv_size == tp_size and tp_size >= 2 and tp_size & (tp_size - 1) == 0
+    lanes = 128 * tp_size
+    return powers and (width // kv_size) % lanes == 0 and out_width % lanes == 0
 
 
 def reduce_tiles(partial, axis_name, axis):
@@ -114,11 +555,16 @@
         (normed * norm_gain.astype(jnp.float32)).astype(jnp.bfloat16).reshape(row_count, width)
     )
     query_width = w_query.shape[1]
-    combined = jnp.concatenate([w_query, w_key, w_value], axis=1)
-    received = lax.all_to_all(normed_rows, "kv", split_axis=1, concat_axis=0, tiled=True)
-    summed = reduce_tiles(
-        jnp.dot(received, combined, preferred_element_type=jnp.float32), "kv", 0
-    )
+    kv_size, tp_size = lax.axis_size("kv"), lax.axis_size("tp")
+    own_kernels = kernels_fit(kv_size, tp_size, width, w_out.shape[1])
+    if own_kernels:
+        summed = project(normed_rows, w_query, w_key, w_value, kv_size, tp_size)
+    else:
+        combined = jnp.concatenate([w_query, w_key, w_value], axis=1)
+        received = lax.all_to_all(normed_rows, "kv", split_axis=1, concat_axis=0, tiled=True)
+        summed = reduce_tiles(
+            jnp.dot(received, combined, preferred_element_type=jnp.float32), "kv", 0
+        )
     query_sum = summed[:, :query_width]
     key_sum = summed[:, query_width : 2 * query_width]
     value_sum = summed[:, 2 * query_width :]
@@ -150,10 +596,15 @@
         forget_pre,
     )
     hidden = head_norm(cell, head_gain)
-    partial_out = jnp.dot(
-        hidden, lax.all_gather(w_out, "kv", axis=1, tiled=True), preferred_element_type=jnp.float32
-    )
-    mixed = reduce_tiles(partial_out, "tp", 1)
+    if own_kernels:
+        mixed = output(hidden, w_out, kv_size, tp_size)
+    else:
+        partial_out = jnp.dot(
+            hidden,
+            lax.all_gather(w_out, "kv", axis=1, tiled=True),
+            preferred_element_type=jnp.float32,
+        )
+        mixed = reduce_tiles(partial_out, "tp", 1)
     return (mixed.reshape(seq_count, props, -1), new_matrix, new_normer, new_stabil)
 
 

time: 188 us -> 111 us (0.59)
  waiting for transfers between devices: 104 us -> 0 us
  Pallas kernels: 0 us -> 82 us
  blocking collectives: 20 us -> 0 us
  between operations: 14.4 us -> 0.94 us
  matrix products: 19.7 us -> 7.55 us
  starting transfers between devices: 10.1 us -> 0 us
    all_to_all x2 -> x0, waiting for transfers between devices: 104 us -> none  [the longest x1 61.7 us: reduce_tiles(): lax.all_to_all(split, axis_name, split_axis=0, concat_axis=0, tiled=True)]
    pallas_call x0 -> x2, Pallas kernels: none -> 82 us  [the longest x1 49.9 us: project(): pl.pallas_call(functools.partial(project_kernel, kv_size, tp_size, chunks...]
    all_to_all x1 -> x0, blocking collectives: 20 us -> none  [reduce_tiles(): lax.all_to_all(split, axis_name, split_axis=0, concat_axis=0, tiled=True)]
    all_to_all x2 -> x0, starting transfers between devices: 10.1 us -> none  [the longest x1 5.41 us: body(): lax.all_to_all(normed_rows, 'kv', split_axis=1, concat_axis=0, tiled=True)]
    dot_general x2 -> x0, matrix products: 7 us -> none  [the longest x1 4.06 us: body(): jnp.dot(received, combined, preferred_element_type=jnp.float32)]
    dot_general x4, matrix products: 11.9 us -> 6.73 us  [bf_dot(): jnp.einsum(spec, left.astype(jnp.bfloat16), right.astype(jnp.bfloat16), p...]
    all_to_all x3 -> x0, local copies, waits for them, and re-layouts: 3.94 us -> none  [body(): lax.all_to_all(normed_rows, 'kv', split_axis=1, concat_axis=0, tiled=True)]
    unnamed x33 -> x27, local copies, waits for them, and re-layouts: 1.47 us -> 3.95 us
  transfers between devices with their start and end apart: 3 -> 0, of which waited for: 2 -> 0; matrix products, arithmetic and copies ran while one was open for 13% -> 0% of each run, Pallas kernels for 0% -> 0%
where the time goes in v1:
time: 111 us; the launch traced here: 110 us
  Pallas kernels  82 us (74%)
  local copies, waits for them, and re-layouts  10.9 us (10%)
  other arithmetic  8.48 us (8%)
  matrix products  7.55 us (7%)
    pallas_call x1, Pallas kernels, project(): pl.pallas_call(functools.partial(project_kernel, kv_size, tp_size, chunks...  49.9 us
    pallas_call x1, Pallas kernels, output(): pl.pallas_call(functools.partial(output_kernel, kv_size, tp_size, stages)...  32.2 us
    dot_general x4, matrix products, bf_dot(): jnp.einsum(spec, left.astype(jnp.bfloat16), right.astype(jnp.bfloat16), p...  6.73 us
    unnamed x27, local copies, waits for them, and re-layouts  3.95 us

profile of v1, /device:TPU:1, one launch (start us, length us, event | category | flops | bytes accessed | tf_op | source)
XLA Modules:
  0.0 109.9 jit_solution(5080726101449760909)
XLA Ops:
  0.7 0.8 iota_compare_fusion.1
  1.4 0.7 convert_element_type.86
  2.1 1.6 %fusion.2 = f32[22,6]{0,1:T(8,128)S(1)} fusion(bf16[22,6,4096]{2,0,1:T(8,128)(2,1)} %param.19), kind=kLoop, calls=%fused_computation.5 | loop fusion | flops 1621884 | bytes 1081872 | tf_op jit(solution)/shard_map/reduce_sum | solution.py:553
  3.7 0.7 fusion.30
  4.5 0.7 fusion.56
  5.2 0.1 copy.163
  5.3 0.1 copy.134
  5.4 0.8 copy.135
  6.2 0.1 copy.137
  6.3 0.7 convert_element_type.70
  7.0 1.0 convert_element_type.75
  7.9 1.0 reshape.125
  9.0 0.4 fusion.4
  9.3 0.6 copy.132
  10.0 0.4 reshape.120.normed_ref
  10.4 0.4 convolution_add_fusion
  10.8 0.4 fusion.5
  11.2 0.1 copy-done.2
  11.4 49.9 %shard_map.210 = bf16[132,1536]{1,0:T(8,128)(2,1)} custom-call(bf16[132,4096]{1,0:T(8,128)(2,1)} %copy-done.2, bf16[1024,512]{1,0:T(8,128)(2,1)} %wq_ref.1, bf16[1024,512]{1,0:T(8,128)(2,1)} %wk_ref.1, bf16[1024,512]{1,0:T(8,128)(2,1)} %wv_ref.1), custom_call_target="tpu_custom_call" | custom-call | tf_op jit(solution)/shard_map/pallas_call | solution.py:235
  61.2 0.1 neg.42
  61.3 0.1 copy.133
  61.5 0.1 copy.138
  61.6 0.1 reshape.121
  61.7 0.3 fusion.10
  62.0 0.1 copy.141
  62.1 0.1 copy.145
  62.2 0.2 fusion.8
  62.5 0.1 multiply_add_fusion.1
  62.6 0.1 copy.149
  62.7 0.9 multiply_convert_fusion.1
  63.6 1.0 fusion.59
  64.7 0.4 fusion.60
  65.1 0.1 copy.153
  65.2 0.2 multiply_reduce_fusion.1
  65.4 0.1 copy.152
  65.6 0.1 copy.158
  65.8 0.1 copy.142
  65.9 0.1 copy.155
  66.0 0.1 copy.154
  66.2 5.0 %multiply_add_fusion = f32[22,4,128,128]{3,2,1,0:T(8,128)S(1)} fusion(f32[22,4,128,128]{3,2,1,0:T(8,128)} %param.30, f32[22,4]{1,0:T(8,128)S(1)} %get-tuple-element.30, f32[22,6,4,128]{3,2,0,1:T(4,128)S(1)} %reshape.125, bf16[22,6,4,128]{3,2,0,1:T(4,128)(2,1)S(1)} %convert_element_type.75, f32[22,4,6]{2,1,0:T(4,128)S(1)} %copy.145), kind=kOutput, calls=%fused_computation | convolution fusion | flops 20320256 | bytes 11942304 | tf_op jit(solution)/shard_map/bhtd,bhte->bhde/dot_general | solution.py:462
  71.1 0.9 fusion
  72.0 1.7 %copy-done.1 = f32[22,4,128,128]{3,2,1,0:T(8,128)} copy-done((f32[22,4,128,128]{3,2,1,0:T(8,128)}, f32[22,4,128,128]{3,2,1,0:T(8,128)S(1)}, u32[]{:S(2)}) %copy-start.1) | copy-done | bytes 5767192
  73.7 0.5 multiply_reduce_fusion
  74.2 0.3 fusion.7
  74.7 0.7 multiply_convert_fusion.hidden_ref
  75.4 32.2 %shard_map.211 = f32[132,1024]{1,0:T(8,128)} custom-call(bf16[132,512]{1,0:T(8,128)(2,1)} %multiply_convert_fusion.hidden_ref, bf16[512,1024]{1,0:T(8,128)(2,1)} %w_ref.1), custom_call_target="tpu_custom_call" | custom-call | tf_op jit(solution)/shard_map/pallas_call | solution.py:418
  107.6 1.1 %reshape.124 = f32[22,6,1024]{2,1,0:T(8,128)S(1)} reshape(f32[132,1024]{1,0:T(8,128)} %shard_map.211) | data formatting | bytes 1081344 | tf_op jit(solution)/shard_map/reshape | solution.py:608
  108.7 1.1 %copy.160 = f32[22,6,1024]{2,0,1:T(8,128)} copy(f32[22,6,1024]{2,1,0:T(8,128)S(1)} %reshape.124) | data formatting | bytes 1081344
  (36 shorter events, 0.5 us)
Async XLA Ops:
  0.6 9.7 %copy-start = (bf16[4096,4]{0,1:T(4,128)(2,1)S(1)}, bf16[4096,4]{0,1:T(4,128)(2,1)}, u32[]{:S(2)}) copy-start(bf16[4096,4]{0,1:T(4,128)(2,1)} %param.24) | copy-start | bytes 98308
  0.6 8.3 %copy-start.3 = (bf16[22,6,4096]{2,0,1:T(8,128)(2,1)S(1)}, bf16[22,6,4096]{2,0,1:T(8,128)(2,1)}, u32[]{:S(2)}) copy-start(bf16[22,6,4096]{2,0,1:T(8,128)(2,1)} %param.19) | copy-start | bytes 3244036
  6.3 59.3 %copy-start.8 = (f32[22,4]{0,1:T(4,128)}, f32[22,4]{0,1:T(4,128)S(1)}, u32[]{:S(2)}) copy-start(f32[22,4]{0,1:T(4,128)S(1)} %copy.137) | copy-start | bytes 1060
  9.3 1.0 copy-start.9
  10.0 0.8 copy-start.7
  10.0 0.8 copy-start.10
  10.4 1.0 copy-start.2
  11.4 50.7 %copy-start.5 = (f32[22,6,4]{0,2,1:T(4,128)S(1)}, f32[22,6,4]{0,2,1:T(4,128)}, u32[]{:S(2)}) copy-start(f32[22,6,4]{0,2,1:T(4,128)} %param.35) | copy-start | bytes 6340
  11.4 51.1 %copy-start.6 = (f32[22,4,128]{2,1,0:T(4,128)S(1)}, f32[22,4,128]{2,1,0:T(4,128)}, u32[]{:S(2)}) copy-start(f32[22,4,128]{2,1,0:T(4,128)} %param.31) | copy-start | bytes 135172
  62.6 3.1 %copy-start.4 = (f32[22,4,128]{2,1,0:T(4,128)}, f32[22,4,128]{2,1,0:T(4,128)S(1)}, u32[]{:S(2)}) copy-start(f32[22,4,128]{2,1,0:T(4,128)S(1)} %multiply_add_fusion.1) | copy-start | bytes 135172
  71.1 2.5 %copy-start.1 = (f32[22,4,128,128]{3,2,1,0:T(8,128)}, f32[22,4,128,128]{3,2,1,0:T(8,128)S(1)}, u32[]{:S(2)}) copy-start(f32[22,4,128,128]{3,2,1,0:T(8,128)S(1)} %multiply_add_fusion) | copy-start | bytes 17301508

commit v2 on v0

--- a/solution.py
+++ b/solution.py
@@ -1,9 +1,658 @@
+import functools
+
 import jax
 import jax.numpy as jnp
 from jax import lax
+from jax.experimental import pallas as pl
+from jax.experimental.pallas import tpu as pltpu
 from jax.sharding import PartitionSpec as P
 
 EPS = 1e-06
+MESH = pl.DeviceIdType.MESH
+
+
+def greet_all(kv_size, tp_size):
+    z, t = lax.axis_index("kv"), lax.axis_index("tp")
+    barrier = pltpu.get_barrier_semaphore()
+    for dz in range(kv_size):
+        for dt in range(tp_size):
+            if dz or dt:
+                pl.semaphore_signal(
+                    barrier,
+                    1,
+                    device_id={"kv": lax.rem(z + dz, kv_size), "tp": lax.rem(t + dt, tp_size)},
+                    device_id_type=MESH,
+                )
+    pl.semaphore_wait(barrier, kv_size * tp_size - 1)
+
+
+def other_at(index, z, kv_size):
+    right = kv_size - 1 - z
+    near, far = jnp.minimum(z, right), jnp.maximum(z, right)
+    single = far - near
+    later = index - single
+    both = jnp.where(later % 2 == 0, z + near - later // 2, z - near + later // 2)
+    lone = jnp.where(right > z, z + far - index, z - far + index)
+    return jnp.where(index < single, lone, both)
+
+
+def looked_up(table, *at):
+    if not at:
+        return table
+    picked = looked_up(table[0], *at[1:])
+    for index in range(1, len(table)):
+        picked = jnp.where(at[0] == index, looked_up(table[index], *at[1:]), picked)
+    return picked
+
+
+def send_order(kv_size):
+    def merged(source, j):
+        return 0 < j < kv_size - 1 and abs(source - j) == 2
+
+    def rank(z, j):
+        behind = 2 * z - j
+        waits = 0 <= behind < kv_size and merged(behind, j)
+        return (waits, not merged(z, j), -abs(z - j), j)
+
+    return [
+        sorted((j for j in range(kv_size) if j != z), key=functools.partial(rank, z))
+        for z in range(kv_size)
+    ]
+
+
+def merged_away(source, j, kv_size):
+    inner = jnp.logical_and(j > 0, j < kv_size - 1)
+    return jnp.logical_and(inner, jnp.abs(source - j) == 2)
+
+
+def remote(src, dst, send, recv, kv, tp):
+    return pltpu.make_async_remote_copy(
+        src_ref=src,
+        dst_ref=dst,
+        send_sem=send,
+        recv_sem=recv,
+        device_id={"kv": kv, "tp": tp},
+        device_id_type=MESH,
+    )
+
+
+def log_sigmoid(x):
+    return jnp.minimum(x, 0.0) - jnp.log1p(jnp.exp(-jnp.abs(x)))
+
+
+def step_kernel(sizes, *refs):
+    kv_size, tp_size, seqs, props, heads = sizes
+    (
+        tokens_hbm, gain_ref, wq_hbm, wk_hbm, wv_hbm, wi_ref, wf_ref, ibias_ref, fbias_ref,
+        head_gain_ref, wo_hbm, matrix_hbm, norm_ref, max_ref, keys_hbm, values_hbm,
+        prior_i_ref, prior_f_ref, accepted_ref,
+        out_ref, new_matrix, new_norm_ref, new_max_ref,
+        tokens, normed, rows_in, weights, own_sum, partial, outgoing, incoming, merging,
+        keys, values, matrix, read_matrix, stacked, columns_of, max_of,
+        w_out, hidden_in, sums, outward, landed, *rest,
+    ) = refs
+    stages = tp_size.bit_length() - 1
+    halves = rest[: 2 * stages]
+    (
+        local_sem, state_sem, a_send, a_recv, f_send, f_recv, b_send, b_recv, m_recv,
+        h_send, h_recv, r_send, r_recv, o_send, o_recv,
+    ) = rest[2 * stages :]
+    z, t = lax.axis_index("kv"), lax.axis_index("tp")
+    others = kv_size - 1
+    groups = normed.shape[0]
+    rows = props * 8
+    depth = weights.shape[0]
+    part = depth // tp_size
+    width = wq_hbm.shape[1]
+    key_size = width // heads
+    out_width = w_out.shape[1]
+    piece = out_width // tp_size
+    f32, bf16 = jnp.float32, jnp.bfloat16
+
+    def live_seqs(group):
+        return min(8, seqs - 8 * group)
+
+    def eight(block):
+        missing = 8 - block.shape[0]
+        if missing:
+            block = jnp.concatenate([block, jnp.zeros((missing, block.shape[1]), f32)], axis=0)
+        return block
+
+    def column(at, size):
+        return pl.ds(pl.multiple_of(at, 128), size)
+
+    token_load = pltpu.make_async_copy(tokens_hbm, tokens, local_sem.at[0])
+    weight_loads = [
+        pltpu.make_async_copy(ref, weights.at[:, pl.ds(at * width, width)], local_sem.at[1 + at])
+        for at, ref in enumerate((wq_hbm, wk_hbm, wv_hbm))
+    ]
+    key_load = pltpu.make_async_copy(keys_hbm, keys, local_sem.at[4])
+    value_load = pltpu.make_async_copy(values_hbm, values, local_sem.at[5])
+    out_load = pltpu.make_async_copy(wo_hbm, w_out, local_sem.at[6])
+
+    def state_load(group):
+        part_of = pl.ds(8 * group, live_seqs(group))
+        return pltpu.make_async_copy(matrix_hbm.at[part_of], matrix.at[part_of], state_sem.at[group])
+
+    token_load.start()
+    for load in weight_loads:
+        load.start()
+    key_load.start()
+    value_load.start()
+    for group in range(groups):
+        state_load(group).start()
+    out_load.start()
+    greet_all(kv_size, tp_size)
+
+    def mine(at):
+        return column(at * part, part)
+
+    def first_copy(group, j, source):
+        return remote(
+            normed.at[group, :, column(j * depth + t * part, part)],
+            rows_in.at[source, group, :, mine(t)],
+            a_send.at[group, j],
+            a_recv.at[group, source],
+            j,
+            t,
+        )
+
+    def forward_copy(group, j, at, stage):
+        source = jnp.bitwise_xor(t, at)
+        block = rows_in.at[j, group, :, mine(source)]
+        peer = jnp.bitwise_xor(t, 1 << stage)
+        return remote(
+            block, block, f_send.at[group, j, at, stage], f_recv.at[group, j, source], z, peer
+        )
+
+    def forwards():
+        held = [0]
+        for stage in reversed(range(stages)):
+            yield stage, list(held)
+            held += [at ^ (1 << stage) for at in held]
+
+    def merge_copy(group, j):
+        way = jnp.where(j > z, 1, 0)
+        middle = jnp.where(j > z, z + 1, z - 1)
+        return remote(
+            outgoing.at[j, group],
+            merging.at[way, group],
+            b_send.at[group, j],
+            m_recv.at[group, way],
+            middle,
+            t,
+        )
+
+    def sum_copy(group, j, source):
+        return remote(
+            outgoing.at[j, group],
+            incoming.at[source, group],
+            b_send.at[group, j],
+            b_recv.at[group, source],
+            j,
+            t,
+        )
+
+    def hidden_copy(group, j, source):
+        return remote(
+            hidden_in.at[group, z],
+            hidden_in.at[group, source],
+            h_send.at[group, j],
+            h_recv.at[group, source],
+            j,
+            t,
+        )
+
+    def half_copy(group, stage, j):
+        peer = jnp.bitwise_xor(t, 1 << stage)
+        return remote(
+            halves[2 * stage].at[group, j],
+            halves[2 * stage + 1].at[group, j],
+            r_send.at[group, stage, j],
+            r_recv.at[group, stage, j],
+            z,
+            peer,
+        )
+
+    def final_copy(group, j):
+        return remote(
+            outward.at[group, j],
+            landed.at[group, t],
+            o_send.at[group, j],
+            o_recv.at[group, t],
+            j,
+            z,
+        )
+
+    def each_other(function):
+        def run(index, carry):
+            function(other_at(index, z, kv_size))
+            return carry
+
+        lax.fori_loop(0, others, run, 0)
+
+    gain_rows = gain_ref[...].astype(f32)
+    gain = jnp.concatenate([gain_rows[at : at + 1] for at in range(gain_rows.shape[0])], axis=1)
+
+    def normalize(group):
+        for pair in range(props // 2):
+            done = []
+            for at in (2 * pair, 2 * pair + 1):
+                x = eight(tokens[at, pl.ds(8 * group, live_seqs(group)), :].astype(f32))
+                scale = lax.rsqrt(jnp.mean(x * x, axis=-1, keepdims=True) + EPS)
+                done.append(x * scale * gain)
+            normed[group, pl.ds(16 * pair, 16), :] = jnp.concatenate(done, axis=0).astype(bf16)
+
+    def start_rows(group):
+        each_other(lambda j: first_copy(group, j, z).start())
+
+    def forward_rows(group):
+        def first(j):
+            first_copy(group, z, j).wait_recv()
+            for stage in reversed(range(stages)):
+                forward_copy(group, j, 0, stage).start()
+
+        def later(j):
+            for stage, held in forwards():
+                for at in held[1:]:
+                    forward_copy(group, j, at, stage).wait_recv()
+                    forward_copy(group, j, at, stage).start()
+
+        each_other(first)
+        each_other(later)
+
+    def own_part(group):
+        own_sum[group] = jnp.dot(
+            normed[group, :, column(z * depth, depth)], weights[...], preferred_element_type=f32
+        )
+
+    def send_sums(group):
+        passed_on = {at for _, held in forwards() for at in held}
+        waited_later = [at for at in range(1, tp_size) if at not in passed_on]
+
+        def unit(j):
+            way = jnp.where(j > z, 1, 0)
+            behind = 2 * z - j
+            merges = jnp.logical_and(behind >= 0, behind < kv_size)
+            merges = jnp.logical_and(merges, merged_away(behind, j, kv_size))
+            for at in waited_later:
+                forward_copy(group, j, at, 0).wait_recv()
+            partial[...] = jnp.dot(rows_in[j, group], weights[...], preferred_element_type=f32)
+
+            @pl.when(merges)
+            def _():
+                merge_copy(group, j).wait_recv()
+                partial[...] += merging[way, group].astype(f32)
+
+            outgoing[j, group] = partial[...].astype(bf16)
+            away = merged_away(z, j, kv_size)
+
+            @pl.when(away)
+            def _():
+                merge_copy(group, j).start()
+
+            @pl.when(jnp.logical_not(away))
+            def _():
+                sum_copy(group, j, z).start()
+
+        order = send_order(kv_size)
+
+        def run(index, carry):
+            unit(looked_up(order, z, index))
+            return carry
+
+        lax.fori_loop(0, others, run, 0)
+
+    def fold_weights():
+        stacked[...] = jnp.zeros_like(stacked)
+        accepted = accepted_ref[...]
+        total = jnp.zeros((heads, seqs), f32)
+        sums_of, gates = [], []
+        for at in range(props):
+            live = jnp.broadcast_to(at < accepted, (heads, seqs))
+            total = total + jnp.where(live, log_sigmoid(prior_f_ref[at]), 0.0)
+            sums_of.append(total)
+            gates.append(jnp.where(live, prior_i_ref[at], -1e30))
+        logs = [total - b + gate for b, gate in zip(sums_of, gates)]
+        top = functools.reduce(jnp.maximum, logs)
+        carried = total + max_ref[...]
+        new_max = jnp.maximum(carried, top)
+        new_max_ref[...] = new_max
+        lanes = pl.ds(0, seqs)
+        for at, log in enumerate(logs):
+            stacked[0, pl.ds(8 * at, heads), lanes] = jnp.exp(log - new_max)
+        stacked[0, pl.ds(8 * props, heads), lanes] = jnp.exp(carried - new_max)
+        stacked[1, pl.ds(0, heads), lanes] = new_max
+        columns_of[...] = stacked[0].T
+        max_of[...] = stacked[1].T
+
+    def fold(group):
+        state_load(group).wait()
+        live = live_seqs(group)
+        here = pl.ds(8 * group, live)
+        row_of = lax.broadcasted_iota(jnp.int32, (rows, 1), 0) % 8
+        table = columns_of[pl.ds(8 * group, 8), :]
+        for head in range(heads):
+            lanes = pl.ds(head * key_size, key_size)
+            weighted, seen = [], []
+            for at in range(props):
+                key = eight(keys[at, here, lanes].astype(f32)) * key_size**-0.5
+                weighted.append(key * table[:, 8 * at + head : 8 * at + head + 1])
+                seen.append(eight(values[at, here, lanes].astype(f32)))
+            carry = table[:, 8 * props + head : 8 * props + head + 1]
+            normer = carry[:live] * norm_ref[here, head, :]
+            new_norm_ref[here, head, :] = normer + sum(weighted)[:live]
+            left = jnp.concatenate(weighted, axis=0).astype(bf16)
+            value = jnp.concatenate(seen, axis=0)
+            spread = jnp.concatenate(
+                [jnp.where(row_of == s, value, 0.0).astype(bf16) for s in range(live)], axis=1
+            )
+            added = lax.dot_general(
+                left, spread, (((0,), (0,)), ((), ())), preferred_element_type=f32
+            )
+            for s in range(live):
+                fresh = carry[s : s + 1] * matrix[8 * group + s, head]
+                fresh = fresh + added[:, s * key_size : (s + 1) * key_size]
+                new_matrix[8 * group + s, head] = fresh
+                read_matrix[group, head, :, pl.ds(s * key_size, key_size)] = fresh.astype(bf16)
+
+    def read(group):
+        def add(j):
+            @pl.when(jnp.logical_not(merged_away(j, z, kv_size)))
+            def _():
+                sum_copy(group, z, j).wait_recv()
+                own_sum[group] += incoming[j, group].astype(f32)
+
+        each_other(add)
+        live = live_seqs(group)
+        rows_of_seq = lax.broadcasted_iota(jnp.int32, (8, 1), 0)
+        contract = (((1,), (1,)), ((), ()))
+        in_pre = lax.dot_general(normed[group], wi_ref[...], contract, preferred_element_type=f32)
+        forget = lax.dot_general(normed[group], wf_ref[...], contract, preferred_element_type=f32)
+        in_pre = in_pre + ibias_ref[...]
+        forget = log_sigmoid(forget + fbias_ref[...])
+        steps = range(props)
+        gate = [in_pre[8 * at : 8 * at + 8] for at in steps]
+        total, b = jnp.zeros((8, heads), f32), []
+        for at in steps:
+            total = total + forget[8 * at : 8 * at + 8]
+            b.append(total)
+        top = max_of[pl.ds(8 * group, 8), :][:, :heads]
+        decay, inter, floor = {}, [], []
+        for at in steps:
+            logs = [b[at] - b[u] + gate[u] for u in range(at + 1)]
+            row_max = functools.reduce(jnp.maximum, logs, b[at] + top)
+            inter.append(jnp.exp(b[at] + top - row_max))
+            floor.append(jnp.exp(-row_max))
+            for u in range(at + 1):
+                decay[at, u] = jnp.exp(logs[u] - row_max)
+        hidden = []
+        for head in range(heads):
+            one = slice(head, head + 1)
+
+            def rounded(kind, head=head):
+                lanes = pl.ds(kind * width + head * key_size, key_size)
+                return own_sum[group, :, lanes].astype(bf16)
+
+            def by_step(array):
+                array = array.astype(f32)
+                return [array[8 * at : 8 * at + 8] for at in steps]
+
+            query_rows = rounded(0)
+            query, key, value = by_step(query_rows), by_step(rounded(1)), by_step(rounded(2))
+            held = live * key_size
+            inward = jnp.dot(
+                query_rows, read_matrix[group, head, :, pl.ds(0, held)], preferred_element_type=f32
+            )
+            normer = eight(new_norm_ref[pl.ds(8 * group, live), head, :])
+            done = []
+            for at in steps:
+                picked = jnp.zeros((8, key_size), f32)
+                for s in range(live):
+                    block = inward[8 * at : 8 * at + 8, s * key_size : (s + 1) * key_size]
+                    picked = jnp.where(rows_of_seq == s, block, picked)
+                scale = inter[at][:, one]
+                numerator = scale * picked
+                denominator = scale * jnp.sum(query[at] * normer, axis=-1, keepdims=True)
+                for u in range(at + 1):
+                    score = jnp.sum(query[at] * key[u], axis=-1, keepdims=True) * key_size**-0.5
+                    score = score * decay[at, u][:, one]
+                    numerator = numerator + score * value[u]
+                    denominator = denominator + score
+                cell = numerator / jnp.maximum(jnp.abs(denominator), floor[at][:, one])
+                mean = jnp.mean(cell * cell, axis=-1, keepdims=True)
+                head_scale = head_gain_ref[pl.ds(head, 1), :].astype(f32)
+                done.append(cell * lax.rsqrt(mean + EPS) * head_scale)
+            hidden.append(jnp.concatenate(done, axis=0).astype(bf16))
+        for head in range(heads):
+            hidden_in[group, z, :, pl.ds(head * key_size, key_size)] = hidden[head]
+        each_other(lambda j: hidden_copy(group, j, z).start())
+
+    def bit_of(stage):
+        return jnp.bitwise_and(lax.shift_right_logical(t, stage), 1)
+
+    def kept_at(stage):
+        return sum(bit_of(at) * (out_width >> (at + 1)) for at in range(stage))
+
+    def split(group, stage, j):
+        half = out_width >> (stage + 1)
+        away = kept_at(stage) + (1 - bit_of(stage)) * half
+        halves[2 * stage][group, j] = sums[group, j, :, column(away, half)].astype(bf16)
+        half_copy(group, stage, j).start()
+
+    def each_near(function):
+        def run(index, carry):
+            other = other_at(jnp.minimum(others - index, others - 1), z, kv_size)
+            function(jnp.where(index == 0, z, other))
+            return carry
+
+        lax.fori_loop(0, kv_size, run, 0)
+
+    def multiply(group):
+        def one(j):
+            @pl.when(j != z)
+            def _():
+                hidden_copy(group, z, j).wait_recv()
+
+            sums[group, j] = jnp.dot(hidden_in[group, j], w_out[...], preferred_element_type=f32)
+            split(group, 0, j)
+
+        each_near(one)
+
+    def reduce(group, stage):
+        def one(j):
+            half_copy(group, stage, j).wait_recv()
+            kept = column(kept_at(stage + 1), out_width >> (stage + 1))
+            sums[group, j, :, kept] += halves[2 * stage + 1][group, j].astype(f32)
+            if stage + 1 < stages:
+                split(group, stage + 1, j)
+                return
+            outward[group, j] = sums[group, j, :, kept].astype(bf16)
+
+            @pl.when(jnp.logical_or(j != z, t != z))
+            def _():
+                final_copy(group, j).start()
+
+        each_near(one)
+
+    def finish(group):
+        live = live_seqs(group)
+        for sender in range(tp_size):
+            at = sum(((sender >> stage) & 1) * (out_width >> (stage + 1)) for stage in range(stages))
+            local = jnp.logical_and(z == t, t == sender)
+
+            @pl.when(local)
+            def _(sender=sender):
+                landed[group, sender] = outward[group, z]
+
+            @pl.when(jnp.logical_not(local))
+            def _(sender=sender):
+                block = landed.at[group, sender]
+                remote(block, block, o_send.at[group, 0], o_recv.at[group, sender], z, t).wait_recv()
+
+            block = landed[group, sender].astype(f32)
+            for step in range(props):
+                out_ref[step, pl.ds(8 * group, live), pl.ds(at, piece)] = block[
+                    8 * step : 8 * step + live
+                ]
+
+    def drain(group):
+        def other(j):
+            first_copy(group, j, z).wait_send()
+            for stage, held in forwards():
+                for at in held:
+                    forward_copy(group, j, at, stage).wait_send()
+            sum_copy(group, j, z).wait_send()
+            hidden_copy(group, j, z).wait_send()
+
+        each_other(other)
+        for j in range(kv_size):
+            for stage in range(stages):
+                half_copy(group, stage, j).wait_send()
+
+            @pl.when(jnp.logical_or(j != z, t != z))
+            def _(j=j):
+                final_copy(group, j).wait_send()
+
+
+    token_load.wait()
+    for group in range(groups):
+        normalize(group)
+        start_rows(group)
+    fold_weights()
+    for load in weight_loads:
+        load.wait()
+    key_load.wait()
+    value_load.wait()
+    own_part(0)
+    fold(0)
+    out_load.wait()
+    for group in range(groups + 3):
+        if group < groups:
+            forward_rows(group)
+            send_sums(group)
+        if 0 < group < groups:
+            own_part(group)
+            fold(group)
+        if 1 <= group <= groups:
+            read(group - 1)
+        if 2 <= group <= groups + 1:
+            multiply(group - 2)
+            for stage in range(stages):
+                reduce(group - 2, stage)
+        if group >= 3:
+            finish(group - 3)
+    for group in range(groups):
+        drain(group)
+
+
+def step(
+    tokens, norm_gain, w_query, w_key, w_value, w_igate, w_fgate, igate_bias, fgate_bias, head_gain,
+    w_out, state_matrix, state_norm, state_max, prior_keys, prior_values, prior_igate, prior_fgate,
+    accepted, kv_size, tp_size,
+):
+    seqs, props, features = tokens.shape
+    heads, key_size = state_matrix.shape[1:3]
+    depth, width = w_query.shape
+    out_width = w_out.shape[1]
+    groups = -(-seqs // 8)
+    rows = 8 * props
+    stages = tp_size.bit_length() - 1
+    piece = out_width // tp_size
+    f32, bf16 = jnp.float32, jnp.bfloat16
+    sem = pltpu.SemaphoreType.DMA
+    hbm = pl.BlockSpec(memory_space=pl.ANY)
+    vmem = pl.BlockSpec(memory_space=pltpu.VMEM)
+    halves = []
+    for stage in range(stages):
+        halves += [pltpu.VMEM((groups, kv_size, rows, out_width >> (stage + 1)), bf16)] * 2
+    by_step = (1, 0, 2)
+    mixed, new_matrix, new_norm, new_max = pl.pallas_call(
+        functools.partial(step_kernel, (kv_size, tp_size, seqs, props, heads)),
+        out_shape=(
+            jax.ShapeDtypeStruct((props, seqs, out_width), f32),
+            pltpu.VMEM(state_matrix.shape, f32),
+            jax.ShapeDtypeStruct(state_norm.shape, f32),
+            jax.ShapeDtypeStruct((heads, seqs), f32),
+        ),
+        in_specs=[hbm, vmem, hbm, hbm, hbm, vmem, vmem, vmem, vmem, vmem, hbm, hbm, vmem, vmem]
+        + [hbm, hbm, vmem, vmem, vmem],
+        out_specs=(vmem, vmem, vmem, vmem),
+        scratch_shapes=[
+            pltpu.VMEM((props, seqs, features), bf16),
+            pltpu.VMEM((groups, rows, features), bf16),
+            pltpu.VMEM((kv_size, groups, rows, depth), bf16),
+            pltpu.VMEM((depth, 3 * width), bf16),
+            pltpu.VMEM((groups, rows, 3 * width), f32),
+            pltpu.VMEM((rows, 3 * width), f32),
+            pltpu.VMEM((kv_size, groups, rows, 3 * width), bf16),
+            pltpu.VMEM((kv_size, groups, rows, 3 * width), bf16),
+            pltpu.VMEM((2, groups, rows, 3 * width), bf16),
+            pltpu.VMEM((props, seqs, width), bf16),
+            pltpu.VMEM((props, seqs, width), bf16),
+            pltpu.VMEM(state_matrix.shape, f32),
+            pltpu.VMEM((groups, heads, key_size, 8 * key_size), bf16),
+            pltpu.VMEM((2, 128, 128), f32),
+            pltpu.VMEM((128, 128), f32),
+            pltpu.VMEM((128, 128), f32),
+            pltpu.VMEM((width, out_width), bf16),
+            pltpu.VMEM((groups, kv_size, rows, width), bf16),
+            pltpu.VMEM((groups, kv_size, rows, out_width), f32),
+            pltpu.VMEM((groups, kv_size, rows, piece), bf16),
+            pltpu.VMEM((groups, tp_size, rows, piece), bf16),
+            *halves,
+            sem((7,)),
+            sem((groups,)),
+            sem((groups, kv_size)),
+            sem((groups, kv_size)),
+            sem((groups, kv_size, tp_size, stages)),
+            sem((groups, kv_size, tp_size)),
+            sem((groups, kv_size)),
+            sem((groups, kv_size)),
+            sem((groups, 2)),
+            sem((groups, kv_size)),
+            sem((groups, kv_size)),
+            sem((groups, stages, kv_size)),
+            sem((groups, stages, kv_size)),
+            sem((groups, kv_size)),
+            sem((groups, tp_size)),
+        ],
+        compiler_params=pltpu.CompilerParams(
+            collective_id=0, has_side_effects=True, vmem_limit_bytes=55 * 1024 * 1024
+        ),
+    )(
+        tokens.transpose(by_step),
+        norm_gain.reshape(-1, 128),
+        w_query,
+        w_key,
+        w_value,
+        w_igate.T,
+        w_fgate.T,
+        igate_bias[None, :],
+        fgate_bias[None, :],
+        head_gain.reshape(-1, key_size),
+        w_out,
+        state_matrix,
+        state_norm,
+        state_max.T,
+        prior_keys.transpose(by_step),
+        prior_values.transpose(by_step),
+        prior_igate.transpose(1, 2, 0),
+        prior_fgate.transpose(1, 2, 0),
+        accepted[None, :],
+    )
+    return mixed.transpose(by_step), new_matrix, new_norm, new_max.T
+
+
+def kernel_fits(kv_size, tp_size, tokens, w_query, w_out, state_matrix):
+    seqs, props, width = tokens.shape
+    heads, key_size, value_size = state_matrix.shape[1:]
+    powers = kv_size == tp_size and 2 <= tp_size and tp_size & (tp_size - 1) == 0
+    lanes = 128 * tp_size
+    cut = (width // kv_size) % lanes == 0 and w_out.shape[1] % lanes == 0
+    square = key_size == value_size == 128 and w_query.shape[1] == heads * key_size
+    small = heads <= 8 and 8 * (props + 1) <= 128 and props % 2 == 0 and seqs <= 128
+    return powers and cut and square and small
 
 
 def reduce_tiles(partial, axis_name, axis):
@@ -104,6 +753,13 @@
     prior_fgate,
     accepted,
 ):
+    kv_size, tp_size = lax.axis_size("kv"), lax.axis_size("tp")
+    if kernel_fits(kv_size, tp_size, tokens, w_query, w_out, state_matrix):
+        return step(
+            tokens, norm_gain, w_query, w_key, w_value, w_igate, w_fgate, igate_bias, fgate_bias,
+            head_gain, w_out, state_matrix, state_norm, state_max, prior_keys, prior_values,
+            prior_igate, prior_fgate, accepted, kv_size, tp_size,
+        )
     seq_count, props, width = tokens.shape
     local_heads = state_matrix.shape[1]
     key_size = state_matrix.shape[2]

time: 188 us -> 81.7 us (0.43)
  waiting for transfers between devices: 104 us -> 0 us
  Pallas kernels: 0 us -> 76.3 us
  blocking collectives: 20 us -> 0 us
  matrix products: 19.7 us -> 0 us
  between operations: 14.4 us -> 0.67 us
  starting transfers between devices: 10.1 us -> 0 us
  other arithmetic: 7.25 us -> 0 us
  local copies, waits for them, and re-layouts: 10.9 us -> 4.56 us
    all_to_all x2 -> x0, waiting for transfers between devices: 104 us -> none  [the longest x1 61.7 us: reduce_tiles(): lax.all_to_all(split, axis_name, split_axis=0, concat_axis=0, tiled=True)]
    pallas_call x0 -> x1, Pallas kernels: none -> 76.3 us  [step(): pl.pallas_call(functools.partial(step_kernel, (kv_size, tp_size, seqs, pr...]
    all_to_all x1 -> x0, blocking collectives: 20 us -> none  [reduce_tiles(): lax.all_to_all(split, axis_name, split_axis=0, concat_axis=0, tiled=True)]
    dot_general x8 -> x0, matrix products: 19.7 us -> none  [the longest x4 11.9 us: bf_dot(): jnp.einsum(spec, left.astype(jnp.bfloat16), right.astype(jnp.bfloat16), p...]
    all_to_all x2 -> x0, starting transfers between devices: 10.1 us -> none  [the longest x1 5.41 us: body(): lax.all_to_all(normed_rows, 'kv', split_axis=1, concat_axis=0, tiled=True)]
    reduce_sum x5 -> x0, other arithmetic: 3.97 us -> none  [the longest x2 1.93 us: reduce_tiles(): return jnp.sum(got.astype(jnp.float32), axis=0)]
    all_to_all x3 -> x0, local copies, waits for them, and re-layouts: 3.94 us -> none  [body(): lax.all_to_all(normed_rows, 'kv', split_axis=1, concat_axis=0, tiled=True)]
    unnamed x33 -> x10, local copies, waits for them, and re-layouts: 1.47 us -> 4.56 us
  transfers between devices with their start and end apart: 3 -> 0, of which waited for: 2 -> 0; matrix products, arithmetic and copies ran while one was open for 13% -> 0% of each run, Pallas kernels for 0% -> 0%
where the time goes in v2:
time: 81.7 us; the launch traced here: 81.5 us
  Pallas kernels  76.3 us (93%)
  local copies, waits for them, and re-layouts  4.56 us (6%)
    pallas_call x1, Pallas kernels, step(): pl.pallas_call(functools.partial(step_kernel, (kv_size, tp_size, seqs, pr...  76.3 us
    unnamed x10, local copies, waits for them, and re-layouts  4.56 us

profile of v2, /device:TPU:1, one launch (start us, length us, event | category | flops | bytes accessed | tf_op | source)
XLA Modules:
  0.0 81.5 jit_solution(5226591257650274089)
XLA Ops:
  0.6 76.3 %shard_map.210 = (f32[6,22,1024]{2,1,0:T(8,128)}, f32[22,4,128,128]{3,2,1,0:T(8,128)S(1)}, f32[22,4,128]{2,1,0:T(4,128)}, f32[4,22]{1,0:T(4,128)}) custom-call(bf16[6,22,4096]{2,1,0:T(8,128)(2,1)} %bitcast.15, bf16[32,128]{1,0:T(8,128)(2,1)} %bitcast.23, bf16[1024,512]{1,0:T(8,128)(2,1)} %refs_2_.1, bf16[1024,512]{1,0:T(8,128)(2,1)} %refs_3_.1, ...), custom_call_target="tpu_custom_call" | custom-call | tf_op jit(solution)/shard_map/pallas_call | solution.py:570
  76.9 0.0 copy-start
  77.0 0.0 copy-start.1
  77.0 0.0 copy-start.2
  77.0 2.5 %copy.27 = f32[22,4,128,128]{3,2,1,0:T(8,128)} copy(f32[22,4,128,128]{3,2,1,0:T(8,128)S(1)} %get-tuple-element.13) | data formatting | bytes 11534336
  79.5 0.0 copy-done
  79.5 0.8 copy.28
  80.3 0.0 copy-done.1
  80.3 0.6 copy.29
  81.0 0.0 copy-done.2
  81.0 0.6 copy.30
Async XLA Ops:
  76.9 2.6 %copy-start = (f32[6,22,1024]{2,1,0:T(8,128)S(1)}, f32[6,22,1024]{2,1,0:T(8,128)}, u32[]{:S(2)}) copy-start(f32[6,22,1024]{2,1,0:T(8,128)} %get-tuple-element.8) | copy-start | bytes 1622020
  77.0 3.4 %copy-start.1 = (f32[22,4,128]{2,1,0:T(4,128)S(1)}, f32[22,4,128]{2,1,0:T(4,128)}, u32[]{:S(2)}) copy-start(f32[22,4,128]{2,1,0:T(4,128)} %get-tuple-element.22) | copy-start | bytes 135172
  77.0 4.0 %copy-start.2 = (f32[4,22]{1,0:T(4,128)S(1)}, f32[4,22]{1,0:T(4,128)}, u32[]{:S(2)}) copy-start(f32[4,22]{1,0:T(4,128)} %get-tuple-element.11) | copy-start | bytes 1060
